TPU v7x, 512 devices: a whole 4x4x16 slice. The times are simulated.
512 devices in a mesh: sp: 128 (over z, x, core), tp: 4 (over y).
Axes of the slice: x: 4, y: 4, z: 16, core: 2. Of those that a mesh axis runs over, the one named last changes fastest.
Arguments:
- tokens: bfloat16 [16384, 2048], P(('sp', 'tp')), may hold values from -6 to 6
- norm_gain: float32 [2048], replicated, may hold values from 0.1 to 1.9
- w_query: bfloat16 [2048, 512], P(None, 'tp'), may hold values from -0.125 to 0.125
- w_key: bfloat16 [2048, 512], P(None, 'tp'), may hold values from -0.125 to 0.125
- w_value: bfloat16 [2048, 512], P(None, 'tp'), may hold values from -0.125 to 0.125
- score_offset: float32 [8], P('tp'), may hold values from -13 to -3, as said below
- w_out: bfloat16 [512, 2048], P('tp'), may hold values from -0.25 to 0.25
Outputs:
- mixed: bfloat16 [16384, 2048], P(('sp', 'tp'))
Inputs may be any that keep to these rules, and one draw needn't show every extreme that they name: `score_offset`: one offset a head.
All inputs are finite; a program needn't handle non-finite values.
Results may differ from a plain program's by a relative error of at most 0.01.
Values may be sent and summed in bfloat16 or wider, within the bound.
A program may use at most 64 MiB of HBM per device.

v0:
```python
import math
import jax
import jax.numpy as jnp
from jax import lax
from jax.sharding import Mesh
from jax.sharding import PartitionSpec as P

HEAD_DIM = 64
SP = ("sp_0", "sp_1", "sp_2")
SP_TP = ("sp_0", "sp_1", "sp_2", "tp")
RMS_EPS = 1e-06


def in_order(tiles, dim):
    tiles = jnp.moveaxis(tiles, 0, dim)
    dims = tiles.shape
    return tiles.reshape(*dims[:dim], dims[dim] * dims[dim + 1], *dims[dim + 2 :])


def sent_to_all(array, axis):
    copies = jnp.broadcast_to(array, (lax.axis_size(axis), *array.shape))
    return lax.all_to_all(copies, axis, split_axis=0, concat_axis=0, tiled=True)


def collect(array, axis, dim):
    return in_order(sent_to_all(array, axis), dim)


def gather_in_order(array, axes, sequence):
    tiles = array[None]
    for k in sequence:
        tiles = lax.all_gather(tiles, axes[k], axis=0, tiled=True)
    block = [lax.axis_size(axes[k]) for k in reversed(sequence)]
    tiles = tiles.reshape(*block, *array.shape)
    turned = sorted(range(len(sequence)), key=lambda place: sequence[len(sequence) - 1 - place])
    return tiles.transpose(*turned, *range(len(sequence), tiles.ndim)).reshape(-1, *array.shape)


def gather_axes(array, axes, sequence, dim):
    return in_order(gather_in_order(array, axes, sequence), dim)


def cut_along(array, dim, count):
    dims = array.shape
    tiles = array.reshape(*dims[:dim], count, dims[dim] // count, *dims[dim + 1 :])
    return jnp.moveaxis(tiles, dim, 0)


def sent_and_summed(array, axis, dim):
    tiles = cut_along(array, dim, lax.axis_size(axis))
    arrived = lax.all_to_all(tiles, axis, split_axis=0, concat_axis=0, tiled=True)
    return arrived.astype(jnp.float32).sum(axis=0)


def per_device(tokens, norm_gain, w_query, w_key, w_value, score_offset, w_out):
    groups = lax.axis_size("tp")
    tok_rows = tokens.shape[0] * groups
    head_width = w_query.shape[1]
    heads_dev = score_offset.shape[0]
    rows_f32 = collect(tokens, "tp", 0).astype(jnp.float32)
    inv_rms = lax.rsqrt(jnp.mean(rows_f32 * rows_f32, axis=1, keepdims=True) + RMS_EPS)
    normed = (rows_f32 * inv_rms * norm_gain).astype(jnp.bfloat16)
    projected = jnp.concatenate(
        [
            jnp.dot(normed, w_query, preferred_element_type=jnp.float32),
            jnp.dot(normed, w_key, preferred_element_type=jnp.float32),
            jnp.dot(normed, w_value, preferred_element_type=jnp.float32),
        ],
        axis=1,
    ).astype(jnp.bfloat16)
    queries = projected[:, :head_width].reshape(tok_rows, heads_dev, HEAD_DIM)
    key_vals = jnp.stack(
        [projected[:, head_width : 2 * head_width], projected[:, 2 * head_width :]]
    )
    own_index = lax.axis_index(SP)
    query_pos = own_index * tok_rows + jnp.arange(tok_rows, dtype=jnp.int32)
    offsets = score_offset[:, None, None]

    def absorb(running, key_block, key_start):
        totals, log_kept = running
        key_rows = key_block.shape[1]
        key_part = key_block[0].reshape(key_rows, heads_dev, HEAD_DIM)
        value_part = key_block[1].reshape(key_rows, heads_dev, HEAD_DIM)
        key_pos = key_start + jnp.arange(key_rows, dtype=jnp.int32)
        scores = (
            jnp.einsum("qhd,khd->hqk", queries, key_part, preferred_element_type=jnp.float32)
            * HEAD_DIM ** (-0.5)
            + offsets
        )
        earlier = ((key_pos[None, :] < query_pos[:, None]) & (key_pos[None, :] >= 0))[None]
        log_keep = jnp.where(earlier, jax.nn.log_sigmoid(-scores), 0.0)
        suffix = lax.cumsum(log_keep, axis=2, reverse=True) - log_keep + log_kept[:, :, None]
        weights = jnp.where(earlier, jnp.exp(jax.nn.log_sigmoid(scores) + suffix), 0.0).astype(
            jnp.bfloat16
        )
        totals = totals + jnp.einsum(
            "hqk,khd->hqd", weights, value_part, preferred_element_type=jnp.float32
        )
        return (totals, log_kept + jnp.sum(log_keep, axis=2))

    start_state = (
        jnp.zeros((heads_dev, tok_rows, HEAD_DIM), jnp.float32),
        jnp.zeros((heads_dev, tok_rows), jnp.float32),
    )
    all_keys = gather_axes(key_vals, SP, (1, 0, 2), 1)
    total_rows = all_keys.shape[1]
    span_rows = math.gcd(total_rows, 2048)
    span_count = total_rows // span_rows

    def sweep(turn_idx, carried):
        span_start = ((span_count - 1 - turn_idx) * span_rows).astype(jnp.int32)
        key_block = lax.dynamic_slice_in_dim(all_keys, span_start, span_rows, 1)
        return absorb(carried, key_block, span_start)

    finished = lax.fori_loop(0, span_count, sweep, start_state)
    mixed_rows = finished[0].transpose(1, 0, 2).reshape(tok_rows, head_width).astype(jnp.bfloat16)
    return sent_and_summed(
        jnp.dot(mixed_rows, w_out, preferred_element_type=jnp.float32).astype(jnp.bfloat16), "tp", 0
    ).astype(jnp.bfloat16)


def solution(mesh):
    finer = Mesh(mesh.devices.reshape(16, 4, 2, mesh.shape["tp"]), ("sp_0", "sp_1", "sp_2", "tp"))
    placed = (
        P(SP_TP, None),
        P(),
        P(None, "tp"),
        P(None, "tp"),
        P(None, "tp"),
        P("tp"),
        P("tp", None),
    )
    return jax.shard_map(
        per_device, mesh=finer, in_specs=placed, out_specs=P(SP_TP, None), check_vma=False
    )
```

profile of v0, /device:TPU:1, one launch (start us, length us, event | category | flops | bytes accessed | tf_op | source)
XLA Modules:
  0.0 320.8 jit_solution(11479637697951911001)
XLA Ops:
  7.7 11.7 %all_to_all.10 = bf16[4,32,2048]{2,1,0:T(8,128)(2,1)S(1)} all-to-all(bf16[4,32,2048]{2,1,0:T(8,128)(2,1)S(1)} %broadcast_in_dim.56), channel_id=1, replica_groups=mesh['sp_0'=16,'sp_1'=4,'sp_2'=2,'tp'=4] {'tp'}, dimensions={0} | all-to-all | bytes 1048576 | tf_op jit(solution)/shard_map/all_to_all | solution.py:22
  20.5 12.1 %all-gather = bf16[8,128,128]{2,1,0:T(8,128)(2,1)} all-gather(bf16[2,128,128]{2,1,0:T(8,128)(2,1)S(1)} %pad_maximum_fusion), channel_id=2, replica_groups=mesh['sp_0'=16,'sp_1'=4,'sp_2'=2,'tp'=4] {'sp_1'}, dimensions={0}, use_global_device_ids=true | all-gather | bytes 327680 | tf_op jit(solution)/shard_map/all_gather | solution.py:32
  32.7 75.2 %all-gather.4.cloned.1.call-done = bf16[64,2,128,128]{3,2,1,0:T(8,128)(2,1)} async-done(((bf16[4,2,128,128]{3,2,1,0:T(8,128)(2,1)}), bf16[64,2,128,128]{3,2,1,0:T(8,128)(2,1)}) %all-gather.4.cloned.1.call-update) | async-done | bytes 4194320 | tf_op jit(solution)/shard_map/all_gather | solution.py:32
  109.3 37.7 %all-gather.6.cloned.1.call-done = bf16[128,2,128,128]{3,2,1,0:T(8,128)(2,1)} async-done(((bf16[64,2,128,128]{3,2,1,0:T(8,128)(2,1)}), bf16[128,2,128,128]{3,2,1,0:T(8,128)(2,1)}) %all-gather.6.cloned.1.call-update) | async-done | bytes 8388624 | tf_op jit(solution)/shard_map/all_gather | solution.py:32
  147.0 10.3 %copy.27 = bf16[16,4,2,2,128,128]{5,4,3,2,1,0:T(8,128)(2,1)} copy(bf16[16,4,2,2,128,128]{5,4,3,1,0,2:T(8,128)(2,1)} %bitcast.75) | data formatting | bytes 16777216 | tf_op jit(solution)/shard_map/transpose | solution.py:36
  157.3 10.3 %copy.28 = bf16[2,128,128,128]{3,2,1,0:T(8,128)(2,1)} copy(bf16[2,128,128,128]{3,2,0,1:T(8,128)(2,1)} %bitcast.72) | data formatting | bytes 16777216 | tf_op jit(solution)/shard_map/transpose | solution.py:15
  167.7 133.3 %while.16 = (s32[]{:T(128)}, f32[2,128,64]{1,2,0:T(8,128)S(1)}, f32[2,128]{1,0:T(2,128)S(1)}, bf16[2,16384,128]{2,1,0:T(8,128)(2,1)}, bf16[128,2,64]{0,2,1:T(8,1...) while((s32[]{:T(128)}, f32[2,128,64]{1,2,0:T(8,128)S(1)}, ...), condition=%wide.region_5.6_spmd.clone, body=%wide.region_1.5_spmd.clone.sunk | while | flops 218732672 | bytes 37794140 | solution.py:115
  170.9 3.2 fusion.46
  174.1 5.0 %fusion.47 = f32[2,128,16,128]{1,2,3,0:T(8,128)S(1)} fusion(f32[2,128,16,128]{1,3,2,0:T(8,128)S(1)} %bitcast.70), kind=kOutput, calls=%fused_computation.15.clone.1 | output fusion | flops 66584576 | bytes 4194304 | tf_op jit(solution)/shard_map/reduce-window.4
  181.0 3.0 fusion.49
  187.6 3.2 fusion.46
  190.8 5.0 %fusion.47 = f32[2,128,16,128]{1,2,3,0:T(8,128)S(1)} fusion(f32[2,128,16,128]{1,3,2,0:T(8,128)S(1)} %bitcast.70), kind=kOutput, calls=%fused_computation.15.clone.1 | output fusion | flops 66584576 | bytes 4194304 | tf_op jit(solution)/shard_map/reduce-window.4
  197.6 3.0 fusion.49
  204.2 3.2 fusion.46
  207.4 5.0 %fusion.47 = f32[2,128,16,128]{1,2,3,0:T(8,128)S(1)} fusion(f32[2,128,16,128]{1,3,2,0:T(8,128)S(1)} %bitcast.70), kind=kOutput, calls=%fused_computation.15.clone.1 | output fusion | flops 66584576 | bytes 4194304 | tf_op jit(solution)/shard_map/reduce-window.4
  214.3 3.0 fusion.49
  220.9 3.2 fusion.46
  224.1 5.0 %fusion.47 = f32[2,128,16,128]{1,2,3,0:T(8,128)S(1)} fusion(f32[2,128,16,128]{1,3,2,0:T(8,128)S(1)} %bitcast.70), kind=kOutput, calls=%fused_computation.15.clone.1 | output fusion | flops 66584576 | bytes 4194304 | tf_op jit(solution)/shard_map/reduce-window.4
  231.0 3.0 fusion.49
  237.6 3.2 fusion.46
  240.8 5.0 %fusion.47 = f32[2,128,16,128]{1,2,3,0:T(8,128)S(1)} fusion(f32[2,128,16,128]{1,3,2,0:T(8,128)S(1)} %bitcast.70), kind=kOutput, calls=%fused_computation.15.clone.1 | output fusion | flops 66584576 | bytes 4194304 | tf_op jit(solution)/shard_map/reduce-window.4
  247.7 3.0 fusion.49
  254.3 3.2 fusion.46
  257.4 5.0 %fusion.47 = f32[2,128,16,128]{1,2,3,0:T(8,128)S(1)} fusion(f32[2,128,16,128]{1,3,2,0:T(8,128)S(1)} %bitcast.70), kind=kOutput, calls=%fused_computation.15.clone.1 | output fusion | flops 66584576 | bytes 4194304 | tf_op jit(solution)/shard_map/reduce-window.4
  264.3 3.0 fusion.49
  270.9 3.2 fusion.46
  274.1 5.0 %fusion.47 = f32[2,128,16,128]{1,2,3,0:T(8,128)S(1)} fusion(f32[2,128,16,128]{1,3,2,0:T(8,128)S(1)} %bitcast.70), kind=kOutput, calls=%fused_computation.15.clone.1 | output fusion | flops 66584576 | bytes 4194304 | tf_op jit(solution)/shard_map/reduce-window.4
  281.0 3.0 fusion.49
  287.6 3.2 fusion.46
  290.8 5.0 %fusion.47 = f32[2,128,16,128]{1,2,3,0:T(8,128)S(1)} fusion(f32[2,128,16,128]{1,3,2,0:T(8,128)S(1)} %bitcast.70), kind=kOutput, calls=%fused_computation.15.clone.1 | output fusion | flops 66584576 | bytes 4194304 | tf_op jit(solution)/shard_map/reduce-window.4
  297.7 3.0 fusion.49
  301.4 11.9 %all_to_all.11 = bf16[4,32,2048]{2,1,0:T(8,128)(2,1)S(1)} all-to-all(bf16[4,32,2048]{2,1,0:T(8,128)(2,1)S(1)} %bitcast.76), channel_id=1, replica_groups=mesh['sp_0'=16,'sp_1'=4,'sp_2'=2,'tp'=4] {'tp'}, dimensions={0} | all-to-all | bytes 1048576 | tf_op jit(solution)/shard_map/all_to_all | solution.py:51
  (174 shorter events, 47.3 us)
Async XLA Ops:
  6.5 294.5 %copy-start = (bf16[128,2048]{1,0:T(8,128)(2,1)S(1)}, bf16[128,2048]{1,0:T(8,128)(2,1)}, u32[]{:S(2)}) copy-start(bf16[128,2048]{1,0:T(8,128)(2,1)} %param.15) | copy-start | bytes 1572868
  6.5 13.1 %copy-start.5 = (f32[2048]{0:T(1024)S(1)}, f32[2048]{0:T(1024)}, u32[]{:S(2)}) copy-start(f32[2048]{0:T(1024)} %param.10) | copy-start | bytes 24580
  6.5 13.3 %copy-start.2 = (bf16[2048,128]{1,0:T(8,128)(2,1)S(1)}, bf16[2048,128]{1,0:T(8,128)(2,1)}, u32[]{:S(2)}) copy-start(bf16[2048,128]{1,0:T(8,128)(2,1)} %param.13) | copy-start | bytes 1572868
  6.5 13.6 %copy-start.3 = (bf16[2048,128]{1,0:T(8,128)(2,1)S(1)}, bf16[2048,128]{1,0:T(8,128)(2,1)}, u32[]{:S(2)}) copy-start(bf16[2048,128]{1,0:T(8,128)(2,1)} %param.12) | copy-start | bytes 1572868
  6.5 101.4 %all-gather.4.cloned.1.call-start = ((), (), s32[]{:S(2)}) async-start(), calls=%async_computation.2 | async-start | bytes 4456448 | tf_op jit(solution)/shard_map/all_gather | solution.py:32
  32.7 114.3 %all-gather.6.cloned.1.call-start = ((), (), s32[]{:S(2)}) async-start(), calls=%async_computation.3 | async-start | bytes 12582912 | tf_op jit(solution)/shard_map/all_gather | solution.py:32
  107.9 1.0 copy-start.4
  157.3 10.4 %copy-start.6 = (f32[2]{0:T(128)S(1)}, f32[2]{0:T(128)}, u32[]{:S(2)}) copy-start(f32[2]{0:T(128)} %param.14) | copy-start | bytes 28
  179.4 1.6 copy-start.1
  181.0 3.3 %copy-start.7 = (f32[2]{0:T(128)S(1)}, f32[2]{0:T(128)}, u32[]{:S(2)}) copy-start(f32[2]{0:T(128)} %get-tuple-element.313) | copy-start | bytes 28 | tf_op jit(solution)/shard_map/while
  196.0 1.6 copy-start.1
  197.6 3.3 %copy-start.7 = (f32[2]{0:T(128)S(1)}, f32[2]{0:T(128)}, u32[]{:S(2)}) copy-start(f32[2]{0:T(128)} %get-tuple-element.313) | copy-start | bytes 28 | tf_op jit(solution)/shard_map/while
  212.7 1.6 copy-start.1
  214.3 3.3 %copy-start.7 = (f32[2]{0:T(128)S(1)}, f32[2]{0:T(128)}, u32[]{:S(2)}) copy-start(f32[2]{0:T(128)} %get-tuple-element.313) | copy-start | bytes 28 | tf_op jit(solution)/shard_map/while
  229.4 1.6 copy-start.1
  231.0 3.3 %copy-start.7 = (f32[2]{0:T(128)S(1)}, f32[2]{0:T(128)}, u32[]{:S(2)}) copy-start(f32[2]{0:T(128)} %get-tuple-element.313) | copy-start | bytes 28 | tf_op jit(solution)/shard_map/while
  246.1 1.6 copy-start.1
  247.7 3.3 %copy-start.7 = (f32[2]{0:T(128)S(1)}, f32[2]{0:T(128)}, u32[]{:S(2)}) copy-start(f32[2]{0:T(128)} %get-tuple-element.313) | copy-start | bytes 28 | tf_op jit(solution)/shard_map/while
  262.7 1.6 copy-start.1
  264.3 3.3 %copy-start.7 = (f32[2]{0:T(128)S(1)}, f32[2]{0:T(128)}, u32[]{:S(2)}) copy-start(f32[2]{0:T(128)} %get-tuple-element.313) | copy-start | bytes 28 | tf_op jit(solution)/shard_map/while
  279.4 1.6 copy-start.1
  281.0 3.3 %copy-start.7 = (f32[2]{0:T(128)S(1)}, f32[2]{0:T(128)}, u32[]{:S(2)}) copy-start(f32[2]{0:T(128)} %get-tuple-element.313) | copy-start | bytes 28 | tf_op jit(solution)/shard_map/while
  296.1 1.6 copy-start.1
  297.7 3.3 %copy-start.7 = (f32[2]{0:T(128)S(1)}, f32[2]{0:T(128)}, u32[]{:S(2)}) copy-start(f32[2]{0:T(128)} %get-tuple-element.313) | copy-start | bytes 28 | tf_op jit(solution)/shard_map/while
Sparse Core Ops, SparseCore 0:
  32.8 75.0 all-gather.3
  110.0 36.9 all-gather.5
where the time goes:
time: 322 us; the launch traced here: 321 us
  waiting for transfers between devices  113 us (35%)
  other arithmetic  79 us (25%)
  local copies, waits for them, and re-layouts  49.2 us (15%)
  blocking collectives  35.7 us (11%)
  matrix products  29.4 us (9%)
  between operations  13.5 us (4%)
    all_gather x2, waiting for transfers between devices, gather_in_order(): tiles = lax.all_gather(tiles, axes[k], axis=0, tiled=True)  113 us
    another operation x16, other arithmetic  40.8 us
    dot_general x8, matrix products, absorb(): jnp.einsum('qhd,khd->hqk', queries, key_part, preferred_element_type=jnp....  25.5 us
    convert_element_type x8, other arithmetic, absorb(): jnp.where(earlier, jnp.exp(jax.nn.log_sigmoid(scores) + suffix), 0.0)  23.9 us
    all_gather x1, blocking collectives, gather_in_order(): tiles = lax.all_gather(tiles, axes[k], axis=0, tiled=True)  12.1 us
    all_to_all x1, blocking collectives, sent_and_summed(): lax.all_to_all(tiles, axis, split_axis=0, concat_axis=0, tiled=True)  11.9 us
    and x8, other arithmetic, absorb(): (key_pos[None, :] < query_pos[:, None]) & (key_pos[None, :] >= 0)  11.8 us
    all_to_all x1, blocking collectives, sent_to_all(): return lax.all_to_all(copies, axis, split_axis=0, concat_axis=0, tiled=True)  11.7 us
  transfers between devices with their start and end apart: 2, of which 2 were waited for; matrix products, arithmetic and copies ran while one was open for 0% of the time, Pallas kernels for 0%

commit v1 on v0

--- a/solution.py
+++ b/solution.py
@@ -29,7 +29,9 @@
 def gather_in_order(array, axes, sequence):
     tiles = array[None]
     for k in sequence:
-        tiles = lax.all_gather(tiles, axes[k], axis=0, tiled=True)
+        tiles = jnp.concatenate(
+            lax.all_to_all(jnp.stack([tiles] * lax.axis_size(axes[k])), axes[k], 0, 0), axis=0
+        )
     block = [lax.axis_size(axes[k]) for k in reversed(sequence)]
     tiles = tiles.reshape(*block, *array.shape)
     turned = sorted(range(len(sequence)), key=lambda place: sequence[len(sequence) - 1 - place])

time: 322 us -> 420 us (1.30)
  waiting for transfers between devices: 113 us -> 181 us
  blocking collectives: 35.7 us -> 53.9 us
  starting transfers between devices: 0.08 us -> 15.1 us
  between operations: 13.5 us -> 0.16 us
  other arithmetic: 79 us -> 86.4 us
    all_to_all x0 -> x1, waiting for transfers between devices: none -> 181 us  [gather_in_order(): lax.all_to_all(jnp.stack([tiles] * lax.axis_size(axes[k])), axes[k], 0, 0)]
    all_gather x2 -> x0, waiting for transfers between devices: 113 us -> none  [gather_in_order(): tiles = lax.all_gather(tiles, axes[k], axis=0, tiled=True)]
    all_to_all x0 -> x2, blocking collectives: none -> 30.6 us  [gather_in_order(): lax.all_to_all(jnp.stack([tiles] * lax.axis_size(axes[k])), axes[k], 0, 0)]
    all_to_all x0 -> x1, starting transfers between devices: none -> 15.1 us  [gather_in_order(): lax.all_to_all(jnp.stack([tiles] * lax.axis_size(axes[k])), axes[k], 0, 0)]
    another operation x16 -> x19, local copies, waits for them, and re-layouts: 0.08 us -> 13.4 us  [the longest x1 10.3 us: gather_in_order(): tiles = tiles.reshape(*block, *array.shape)]
    all_gather x1 -> x0, blocking collectives: 12.1 us -> none  [gather_in_order(): tiles = lax.all_gather(tiles, axes[k], axis=0, tiled=True)]
    transpose x1 -> x0, local copies, waits for them, and re-layouts: 10.3 us -> none  [gather_in_order(): tiles.transpose(*turned, *range(len(sequence), tiles.ndim))]
    another operation x16 -> x17, other arithmetic: 40.8 us -> 48.2 us
  transfers between devices with their start and end apart: 2 -> 1, of which waited for: 2 -> 1; matrix products, arithmetic and copies ran while one was open for 0% -> 0% of each run, Pallas kernels for 0% -> 0%
where the time goes in v1:
time: 420 us; the launch traced here: 419 us
  waiting for transfers between devices  181 us (43%)
  other arithmetic  86.4 us (21%)
  blocking collectives  53.9 us (13%)
  local copies, waits for them, and re-layouts  51.2 us (12%)
  matrix products  29.7 us (7%)
  starting transfers between devices  15.1 us (4%)
    all_to_all x1, waiting for transfers between devices, gather_in_order(): lax.all_to_all(jnp.stack([tiles] * lax.axis_size(axes[k])), axes[k], 0, 0)  181 us
    another operation x16, other arithmetic  40.8 us
    all_to_all x2, blocking collectives, gather_in_order(): lax.all_to_all(jnp.stack([tiles] * lax.axis_size(axes[k])), axes[k], 0, 0)  30.6 us
    dot_general x8, matrix products, absorb(): jnp.einsum('qhd,khd->hqk', queries, key_part, preferred_element_type=jnp....  25.8 us
    convert_element_type x8, other arithmetic, absorb(): jnp.where(earlier, jnp.exp(jax.nn.log_sigmoid(scores) + suffix), 0.0)  23.9 us
    all_to_all x1, starting transfers between devices, gather_in_order(): lax.all_to_all(jnp.stack([tiles] * lax.axis_size(axes[k])), axes[k], 0, 0)  15.1 us
    and x8, other arithmetic, absorb(): (key_pos[None, :] < query_pos[:, None]) & (key_pos[None, :] >= 0)  11.8 us
    all_to_all x1, blocking collectives, sent_to_all(): return lax.all_to_all(copies, axis, split_axis=0, concat_axis=0, tiled=True)  11.7 us
  transfers between devices with their start and end apart: 1, of which 1 were waited for; matrix products, arithmetic and copies ran while one was open for 0% of the time, Pallas kernels for 0%

profile of v1, /device:TPU:1, one launch (start us, length us, event | category | flops | bytes accessed | tf_op | source)
XLA Modules:
  0.0 419.0 jit_solution(4414463520227936977)
XLA Ops:
  1.1 11.7 %all_to_all.25 = bf16[4,32,2048]{2,1,0:T(8,128)(2,1)S(1)} all-to-all(bf16[4,32,2048]{2,1,0:T(8,128)(2,1)S(1)} %broadcast_in_dim.53), channel_id=1, replica_groups=mesh['sp_0'=16,'sp_1'=4,'sp_2'=2,'tp'=4] {'tp'}, dimensions={0} | all-to-all | bytes 1048576 | tf_op jit(solution)/shard_map/all_to_all | solution.py:22
  14.0 11.0 %all_to_all.26 = bf16[4,1,2,128,128]{4,3,2,1,0:T(8,128)(2,1)S(1)} all-to-all(bf16[4,1,2,128,128]{4,3,2,1,0:T(8,128)(2,1)S(1)} %stack.21), channel_id=1, replica_groups=mesh['sp_0'=16,'sp_1'=4,'sp_2'=2,'tp'=4] {'sp_1'}, dimensions={0} | all-to-all | bytes 524288 | tf_op jit(solution)/shard_map/all_to_all | solution.py:33
  28.0 15.1 %all-to-all-start.2 = ((bf16[16,4,2,128,128]{4,3,2,1,0:T(8,128)(2,1)}), bf16[16,4,2,128,128]{4,3,2,1,0:T(8,128)(2,1)}, u32[]{:S(2)}, u32[]{:S(2)}) async-start(bf16[16,4,2,128,128]{4,3,2,1,0:T(8,128)(2,1)} %stack.22), calls=%async_computation.2 | async-start | bytes 8388608 | tf_op jit(solution)/shard_map/all_to_all | solution.py:33
  43.5 181.4 %all-to-all-done.2 = bf16[16,4,2,128,128]{4,3,2,1,0:T(8,128)(2,1)} async-done(((bf16[16,4,2,128,128]{4,3,2,1,0:T(8,128)(2,1)}), bf16[16,4,2,128,128]{4,3,2,1,0:T(8,128)(2,1)}, u32[]{:S(2)}, u32[]{:S(2)}) %all-to-all-start.2) | async-done | bytes 4194336 | tf_op jit(solution)/shard_map/all_to_all | solution.py:33
  224.9 7.5 %pad_maximum_fusion = bf16[2,64,2,128,128]{4,3,2,1,0:T(8,128)(2,1)} fusion(bf16[1,64,2,128,128]{4,3,2,1,0:T(8,128)(2,1)} %bitcast.4), kind=kLoop, calls=%fused_computation.28 | loop fusion | flops 4194304 | bytes 12582912 | tf_op jit(solution)/shard_map/stack | solution.py:33
  232.4 19.5 %all_to_all.27 = bf16[2,64,2,128,128]{4,3,2,1,0:T(8,128)(2,1)} all-to-all(bf16[2,64,2,128,128]{4,3,2,1,0:T(8,128)(2,1)} %pad_maximum_fusion), channel_id=1, replica_groups=mesh['sp_0'=16,'sp_1'=4,'sp_2'=2,'tp'=4] {'sp_2'}, dimensions={0} | all-to-all | bytes 16777216 | tf_op jit(solution)/shard_map/all_to_all | solution.py:33
  251.9 10.3 %copy.34 = bf16[2,16,4,2,128,128]{5,4,3,0,2,1:T(8,128)(2,1)} copy(bf16[2,16,4,2,128,128]{5,4,3,2,1,0:T(8,128)(2,1)} %bitcast.73) | data formatting | bytes 16777216 | tf_op jit(solution)/shard_map/reshape;reshape | solution.py:36
  262.3 10.4 %copy.35 = bf16[2,128,128,128]{3,2,1,0:T(8,128)(2,1)} copy(bf16[2,128,128,128]{3,2,0,1:T(8,128)(2,1)} %bitcast.74) | data formatting | bytes 16777216 | tf_op jit(solution)/shard_map/transpose | solution.py:15
  272.6 133.6 %while.16 = (s32[]{:T(128)}, f32[2,128,64]{1,2,0:T(8,128)S(1)}, f32[2,128]{1,0:T(2,128)S(1)}, bf16[2,16384,128]{2,1,0:T(8,128)(2,1)}, bf16[128,2,64]{0,2,1:T(8,1...) while((s32[]{:T(128)}, f32[2,128,64]{1,2,0:T(8,128)S(1)}, ...), condition=%wide.region_5.6_spmd.clone, body=%wide.region_1.5_spmd.clone.sunk | while | flops 218732672 | bytes 37794140 | solution.py:117
  275.8 3.2 fusion.46
  279.1 5.0 %fusion.47 = f32[2,128,16,128]{1,2,3,0:T(8,128)S(1)} fusion(f32[2,128,16,128]{1,3,2,0:T(8,128)S(1)} %bitcast.71), kind=kOutput, calls=%fused_computation.15.clone.1 | output fusion | flops 66584576 | bytes 4194304 | tf_op jit(solution)/shard_map/reduce-window.4
  286.0 3.0 fusion.49
  292.6 3.2 fusion.46
  295.8 5.0 %fusion.47 = f32[2,128,16,128]{1,2,3,0:T(8,128)S(1)} fusion(f32[2,128,16,128]{1,3,2,0:T(8,128)S(1)} %bitcast.71), kind=kOutput, calls=%fused_computation.15.clone.1 | output fusion | flops 66584576 | bytes 4194304 | tf_op jit(solution)/shard_map/reduce-window.4
  302.7 3.0 fusion.49
  309.3 3.2 fusion.46
  312.5 5.0 %fusion.47 = f32[2,128,16,128]{1,2,3,0:T(8,128)S(1)} fusion(f32[2,128,16,128]{1,3,2,0:T(8,128)S(1)} %bitcast.71), kind=kOutput, calls=%fused_computation.15.clone.1 | output fusion | flops 66584576 | bytes 4194304 | tf_op jit(solution)/shard_map/reduce-window.4
  319.4 3.0 fusion.49
  326.0 3.2 fusion.46
  329.2 5.0 %fusion.47 = f32[2,128,16,128]{1,2,3,0:T(8,128)S(1)} fusion(f32[2,128,16,128]{1,3,2,0:T(8,128)S(1)} %bitcast.71), kind=kOutput, calls=%fused_computation.15.clone.1 | output fusion | flops 66584576 | bytes 4194304 | tf_op jit(solution)/shard_map/reduce-window.4
  336.1 3.0 fusion.49
  342.7 3.2 fusion.46
  345.9 5.0 %fusion.47 = f32[2,128,16,128]{1,2,3,0:T(8,128)S(1)} fusion(f32[2,128,16,128]{1,3,2,0:T(8,128)S(1)} %bitcast.71), kind=kOutput, calls=%fused_computation.15.clone.1 | output fusion | flops 66584576 | bytes 4194304 | tf_op jit(solution)/shard_map/reduce-window.4
  352.8 3.0 fusion.49
  359.4 3.2 fusion.46
  362.6 5.0 %fusion.47 = f32[2,128,16,128]{1,2,3,0:T(8,128)S(1)} fusion(f32[2,128,16,128]{1,3,2,0:T(8,128)S(1)} %bitcast.71), kind=kOutput, calls=%fused_computation.15.clone.1 | output fusion | flops 66584576 | bytes 4194304 | tf_op jit(solution)/shard_map/reduce-window.4
  369.5 3.0 fusion.49
  376.1 3.2 fusion.46
  379.3 5.0 %fusion.47 = f32[2,128,16,128]{1,2,3,0:T(8,128)S(1)} fusion(f32[2,128,16,128]{1,3,2,0:T(8,128)S(1)} %bitcast.71), kind=kOutput, calls=%fused_computation.15.clone.1 | output fusion | flops 66584576 | bytes 4194304 | tf_op jit(solution)/shard_map/reduce-window.4
  392.8 3.2 fusion.46
  396.0 5.0 %fusion.47 = f32[2,128,16,128]{1,2,3,0:T(8,128)S(1)} fusion(f32[2,128,16,128]{1,3,2,0:T(8,128)S(1)} %bitcast.71), kind=kOutput, calls=%fused_computation.15.clone.1 | output fusion | flops 66584576 | bytes 4194304 | tf_op jit(solution)/shard_map/reduce-window.4
  406.6 11.6 %all_to_all.28 = bf16[4,32,2048]{2,1,0:T(8,128)(2,1)S(1)} all-to-all(bf16[4,32,2048]{2,1,0:T(8,128)(2,1)S(1)} %bitcast.77), channel_id=1, replica_groups=mesh['sp_0'=16,'sp_1'=4,'sp_2'=2,'tp'=4] {'tp'}, dimensions={0} | all-to-all | bytes 1048576 | tf_op jit(solution)/shard_map/all_to_all | solution.py:53
  (174 shorter events, 55.2 us)
Async XLA Ops:
  0.0 406.3 %copy-start = (bf16[128,2048]{1,0:T(8,128)(2,1)S(1)}, bf16[128,2048]{1,0:T(8,128)(2,1)}, u32[]{:S(2)}) copy-start(bf16[128,2048]{1,0:T(8,128)(2,1)} %param.15) | copy-start | bytes 1572868
  0.0 13.1 %copy-start.5 = (f32[2048]{0:T(1024)S(1)}, f32[2048]{0:T(1024)}, u32[]{:S(2)}) copy-start(f32[2048]{0:T(1024)} %param.10) | copy-start | bytes 24580
  0.0 13.3 %copy-start.2 = (bf16[2048,128]{1,0:T(8,128)(2,1)S(1)}, bf16[2048,128]{1,0:T(8,128)(2,1)}, u32[]{:S(2)}) copy-start(bf16[2048,128]{1,0:T(8,128)(2,1)} %param.13) | copy-start | bytes 1572868
  0.0 13.6 %copy-start.3 = (bf16[2048,128]{1,0:T(8,128)(2,1)S(1)}, bf16[2048,128]{1,0:T(8,128)(2,1)}, u32[]{:S(2)}) copy-start(bf16[2048,128]{1,0:T(8,128)(2,1)} %param.12) | copy-start | bytes 1572868
  28.0 15.1 %copy-start.4 = (bf16[2048,128]{1,0:T(8,128)(2,1)S(1)}, bf16[2048,128]{1,0:T(8,128)(2,1)}, u32[]{:S(2)}) copy-start(bf16[2048,128]{1,0:T(8,128)(2,1)} %param.11) | copy-start | bytes 1572868
  28.0 196.9 %all-to-all-start.2 = ((bf16[16,4,2,128,128]{4,3,2,1,0:T(8,128)(2,1)}), bf16[16,4,2,128,128]{4,3,2,1,0:T(8,128)(2,1)}, u32[]{:S(2)}, u32[]{:S(2)}) async-start(bf16[16,4,2,128,128]{4,3,2,1,0:T(8,128)(2,1)} %stack.22), calls=%async_computation.2 | async-start | bytes 8388608 | tf_op jit(solution)/shard_map/all_to_all | solution.py:33
  262.3 10.4 %copy-start.6 = (f32[2]{0:T(128)S(1)}, f32[2]{0:T(128)}, u32[]{:S(2)}) copy-start(f32[2]{0:T(128)} %param.14) | copy-start | bytes 28
  284.4 1.6 copy-start.1
  285.9 3.3 copy-start.7
  301.1 1.6 copy-start.1
  302.7 3.3 copy-start.7
  317.8 1.6 copy-start.1
  319.4 3.3 copy-start.7
  334.5 1.6 copy-start.1
  336.1 3.3 copy-start.7
  351.2 1.6 copy-start.1
  352.8 3.3 copy-start.7
  367.9 1.6 copy-start.1
  369.5 3.3 copy-start.7
  384.6 1.6 copy-start.1
  386.2 3.3 copy-start.7
  401.3 1.6 copy-start.1
  402.9 3.3 copy-start.7
